TPU v7x, 32 devices: a whole 2x2x4 slice. The times are simulated.
32 devices in a mesh: sp: 8 (over z, x), tp: 4 (over y, core).
Axes of the slice: x: 2, y: 2, z: 4, core: 2. Of those that a mesh axis runs over, the one named last changes fastest.
Arguments:
- token_grid: bfloat16 [8, 2048, 512], P('sp', 'tp'), may hold values from -6 to 6
- norm_gain: bfloat16 [3, 2048], replicated, may hold values from 0.099609375 to 1.8984375
- w_query: bfloat16 [3, 2048, 2048], P(None, None, 'tp'), may hold values from -0.125 to 0.125
- w_key: bfloat16 [3, 2048, 2048], P(None, None, 'tp'), may hold values from -0.125 to 0.125
- w_value: bfloat16 [3, 2048, 2048], P(None, None, 'tp'), may hold values from -0.125 to 0.125
- w_out: bfloat16 [3, 2048, 2048], P(None, 'tp'), may hold values from -0.5 to 0.5
- rel_bias: float32 [3, 32, 8, 16], P(None, 'tp'), may hold values from -3 to 250
Outputs:
- grid_out: bfloat16 [8, 2048, 512], P('sp', 'tp')
All inputs are finite; a program needn't handle non-finite values.
Results may differ from a plain program's by a relative error of at most 0.024.
Values may be sent and summed in bfloat16 or wider, within the bound.
A program may use at most 128 MiB of HBM per device.

v0:
```python
import jax
import jax.numpy as jnp
from jax import lax
from jax.sharding import PartitionSpec as P

D = 2048
HEAD_DIM = 64
WIN_R = 8
WIN_C = 16
LAYERS = 3


EPS = 1e-06


def from_behind(block, axis, distance):
    devices = range(lax.axis_size(axis))
    route = [((i - distance) % len(devices), i) for i in devices]
    return lax.ppermute(block, axis, route)


def periodic(source, columns):
    half_c = WIN_C // 2
    return jnp.concatenate(
        [source[..., columns - half_c :], source, source[..., : WIN_C - half_c - 1]], axis=-1
    )


def body(token_grid, norm_gain, w_query, w_key, w_value, w_out, rel_bias):
    current = token_grid
    heads_dev = rel_bias.shape[1]
    channels = w_query.shape[2]
    columns = token_grid.shape[2]
    half_r = WIN_R // 2
    factor = HEAD_DIM ** (-0.5)
    for layer_idx in range(LAYERS):
        gain_row = norm_gain[layer_idx].astype(jnp.float32)
        rows_query = w_query[layer_idx]
        rows_key = w_key[layer_idx]
        rows_value = w_value[layer_idx]
        raw_rows = lax.all_gather(current, "tp", axis=1, tiled=True)[0].astype(jnp.float32)
        scaled = (raw_rows * gain_row[:, None]).astype(jnp.bfloat16)
        slice_keyval = jnp.concatenate([rows_key, rows_value], axis=1)
        contract = (((0,), (0,)), ((), ()))
        acc_query = lax.dot_general(
            rows_query, scaled, contract, preferred_element_type=jnp.float32
        )
        acc_keyval = lax.dot_general(
            slice_keyval, scaled, contract, preferred_element_type=jnp.float32
        )
        squares = jnp.sum(raw_rows * raw_rows, axis=0)
        acc_query, acc_keyval, squares = (acc_query, acc_keyval, squares)
        inverse = lax.rsqrt(squares / D + EPS)
        queries = (acc_query * inverse[None, :]).astype(jnp.bfloat16)
        keyval = (acc_keyval * inverse[None, :]).astype(jnp.bfloat16)
        rows_list = []
        for slot_idx in range(WIN_R):
            distance = half_r - slot_idx
            if distance == 0:
                rows_list.append(keyval)
            else:
                rows_list.append(from_behind(keyval, "sp", distance))
        window_rows = jnp.stack(rows_list)
        key_rows = window_rows[:, :channels].reshape(WIN_R, heads_dev, HEAD_DIM, columns)
        value_rows = window_rows[:, channels:].reshape(WIN_R, heads_dev, HEAD_DIM, columns)
        query_heads = queries.reshape(heads_dev, HEAD_DIM, columns)
        bias_table = rel_bias[layer_idx]
        wide_keys = periodic(key_rows, columns)
        score_list = []
        for offset in range(WIN_C):
            shifted = wide_keys[..., offset : offset + columns]
            partial_value = jnp.einsum(
                "hdc,shdc->shc", query_heads, shifted, preferred_element_type=jnp.float32
            )
            score_list.append(
                partial_value * factor + jnp.transpose(bias_table[:, :, offset])[:, :, None]
            )
        scores = jnp.stack(score_list)
        highest = jnp.max(scores, axis=(0, 1), keepdims=True)
        weights = jnp.exp(scores - highest)
        weights = (weights / jnp.sum(weights, axis=(0, 1), keepdims=True)).astype(jnp.bfloat16)
        wide_values = periodic(value_rows, columns)
        mixed_out = jnp.zeros((heads_dev, HEAD_DIM, columns), jnp.float32)
        for offset in range(WIN_C):
            shifted = wide_values[..., offset : offset + columns]
            mixed_out = mixed_out + jnp.einsum(
                "shc,shdc->hdc", weights[offset], shifted, preferred_element_type=jnp.float32
            )
        mixed_out = mixed_out.reshape(channels, columns).astype(jnp.bfloat16)
        w_layer = w_out[layer_idx]
        update = lax.psum_scatter(
            lax.dot_general(
                w_layer, mixed_out, (((0,), (0,)), ((), ())), preferred_element_type=jnp.float32
            ).astype(jnp.bfloat16),
            "tp",
            scatter_dimension=0,
            tiled=True,
        ).astype(jnp.float32)
        current = (current[0].astype(jnp.float32) + update).astype(jnp.bfloat16)[None]
    return current


def solution(mesh):
    in_specs = (
        P("sp", "tp", None),
        P(),
        P(None, None, "tp"),
        P(None, None, "tp"),
        P(None, None, "tp"),
        P(None, "tp", None),
        P(None, "tp", None, None),
    )
    out_specs = P("sp", "tp", None)
    return jax.shard_map(body, mesh=mesh, in_specs=in_specs, out_specs=out_specs, check_vma=False)
```

profile of v0, /device:TPU:0, one launch (start us, length us, event | category | flops | bytes accessed | tf_op | source)
XLA Modules:
  0.0 1064.6 jit_solution(12954596138400243531)
XLA Ops:
  7.3 1.4 slice_convert_fusion
  8.7 8.9 slice_bitcast_fusion
  17.7 16.6 %all-gather.6.cloned.1.call-done = bf16[1,2048,512]{2,1,0:T(8,128)(2,1)} async-done(((bf16[1,512,512]{2,1,0:T(8,128)(2,1)}), bf16[1,2048,512]{2,1,0:T(8,128)(2,1)}) %all-gather.6.cloned.1.call-update) | async-done | bytes 2097168 | tf_op jit(solution)/shard_map/all_gather | solution.py:41
  34.2 2.1 fusion.159
  36.3 4.7 multiply_convert_fusion.2
  41.0 2.5 collective-permute-start
  43.5 2.4 collective-permute-start.1
  48.8 3.7 collective-permute-start.4
  52.5 3.7 bitcast_convert_fusion.2
  56.2 79.4 %collective-permute-done = bf16[1024,512]{1,0:T(8,128)(2,1)} collective-permute-done((bf16[1024,512]{1,0:T(8,128)(2,1)S(1)}, bf16[1024,512]{1,0:T(8,128)(2,1)}, u32[]{:S(2)}, u32[]{:S(2)}) %collective-permute-start) | collective-permute-done | bytes 1048608 | tf_op jit(solution)/shard_map/ppermute | solution.py:19
  135.6 1.3 bitcast_dynamic-update-slice_fusion.23
  136.9 44.4 %collective-permute-done.1 = bf16[1024,512]{1,0:T(8,128)(2,1)S(1)} collective-permute-done((bf16[1024,512]{1,0:T(8,128)(2,1)S(1)}, bf16[1024,512]{1,0:T(8,128)(2,1)S(1)}, u32[]{:S(2)}, u32[]{:S(2)}) %collective-permute-start.1) | collective-permute-done | bytes 1048608 | tf_op jit(solution)/shard_map/ppermute | solution.py:19
  182.1 43.4 %collective-permute-done.6 = bf16[1024,512]{1,0:T(8,128)(2,1)S(1)} collective-permute-done((bf16[1024,512]{1,0:T(8,128)(2,1)S(1)}, bf16[1024,512]{1,0:T(8,128)(2,1)S(1)}, u32[]{:S(2)}, u32[]{:S(2)}) %collective-permute-start.6) | collective-permute-done | bytes 1048608 | tf_op jit(solution)/shard_map/ppermute | solution.py:19
  226.7 18.0 %multiply_reduce_fusion.88 = (f32[8,512,8]{1,0,2:T(8,128)S(1)}, f32[8,512,8]{1,0,2:T(8,128)S(1)}, f32[8,512,8]{1,0,2:T(8,128)S(1)}, f32[8,512,8]{1,0,2:T(8,128)S...) fusion(bf16[8,8,64,512]{3,2,1,0:T(8,128)(2,1)S(1)} %bitcast.156, ...), kind=kLoop, calls=%fused_computation.166 | loop fusion | flops 117178368 | bytes 6356992 | tf_op jit(solution)/shard_map/hdc,shdc->shc/dot_general | solution.py:72
  245.5 20.8 %multiply_reduce_fusion.80 = (f32[8,512,8]{1,0,2:T(8,128)S(1)}, f32[8,512,8]{1,0,2:T(8,128)S(1)}, f32[8,512,8]{1,0,2:T(8,128)S(1)}, f32[8,512,8]{1,0,2:T(8,128)S...) fusion(bf16[8,8,64,7]{3,2,1,0:T(8,128)(2,1)S(1)} %slice.1007, ...), kind=kLoop, calls=%fused_computation.158 | loop fusion | flops 108789760 | bytes 10543104 | tf_op jit(solution)/shard_map/hdc,shdc->shc/dot_general | solution.py:72
  270.5 2.1 multiply_reduce_fusion.71
  272.7 9.0 multiply_reduce_fusion.73
  281.6 15.7 %multiply_reduce_fusion.78 = (f32[8,512,64]{1,2,0:T(8,128)}, f32[8,512,64]{1,2,0:T(8,128)}, f32[8,512,64]{1,2,0:T(8,128)}, f32[8,512,64]{1,2,0:T(8,128)}, f32[8,512,64]{1,2,0:T(8,128)}, /*index=5*/f32[8,512,64]{1,2,0:T(8,128)}) fusion(bf16[8,8,64,512]{3,2,1,0:T(8,128)(2,1)S(1)} %bitcast.1552, bf16[8,8,64,8]{3,2,1,0:T(8,128)(2,1)S(1)} %slice.979, ...), kind=kLoop, calls=%fused_computation.156 | loop fusion | flops 86507520 | bytes 11337728 | tf_op jit(solution)/shard_map/shc,shdc->hdc/dot_general | solution.py:86
  297.3 19.1 %multiply_reduce_fusion.70 = (f32[8,512,64]{1,2,0:T(8,128)}, f32[8,512,64]{1,2,0:T(8,128)}, f32[8,512,64]{1,2,0:T(8,128)}, f32[8,512,64]{1,2,0:T(8,128)}, f32[8,512,64]{1,2,0:T(8,128)}, /*index=5*/f32[8,512,64]{1,2,0:T(8,128)}) fusion(bf16[8,8,64,512]{3,2,1,0:T(8,128)(2,1)S(1)} %bitcast.1553, bf16[8,8,64,7]{3,2,1,0:T(8,128)(2,1)S(1)} %slice.1048, ...), kind=kLoop, calls=%fused_computation.148 | loop fusion | flops 86507520 | bytes 11329536 | tf_op jit(solution)/shard_map/shc,shdc->hdc/dot_general | solution.py:86
  316.5 6.4 add_convert_fusion.2
  322.9 4.3 fusion.193
  327.5 30.2 %reduce-scatter.4.cloned.1.call-done = bf16[512,512]{0,1:T(8,128)(2,1)} async-done(((bf16[2048,512]{0,1:T(8,128)(2,1)}), bf16[512,512]{0,1:T(8,128)(2,1)}) %reduce-scatter.4.cloned.1.call-update) | async-done | bytes 524304 | tf_op jit(solution)/shard_map/reduce_scatter | solution.py:91
  357.7 2.0 fusion.271
  359.7 22.7 %all-gather.8.cloned.1.call-done = bf16[2048,512]{0,1:T(8,128)(2,1)} async-done(((bf16[512,512]{0,1:T(8,128)(2,1)}), bf16[2048,512]{0,1:T(8,128)(2,1)}) %all-gather.8.cloned.1.call-update) | async-done | bytes 2097168 | tf_op jit(solution)/shard_map/all_gather | solution.py:41
  382.4 2.1 fusion.161
  384.5 4.6 multiply_convert_fusion.1
  389.1 2.5 collective-permute-start.7
  391.6 2.4 collective-permute-start.8
  396.3 3.7 collective-permute-start.11
  400.0 3.5 bitcast_convert_fusion.1
  403.5 80.2 %collective-permute-done.7 = bf16[1024,512]{1,0:T(8,128)(2,1)} collective-permute-done((bf16[1024,512]{1,0:T(8,128)(2,1)S(1)}, bf16[1024,512]{1,0:T(8,128)(2,1)}, u32[]{:S(2)}, u32[]{:S(2)}) %collective-permute-start.7) | collective-permute-done | bytes 1048608 | tf_op jit(solution)/shard_map/ppermute | solution.py:19
  483.7 1.3 bitcast_dynamic-update-slice_fusion.15
  485.0 44.4 %collective-permute-done.8 = bf16[1024,512]{1,0:T(8,128)(2,1)S(1)} collective-permute-done((bf16[1024,512]{1,0:T(8,128)(2,1)S(1)}, bf16[1024,512]{1,0:T(8,128)(2,1)S(1)}, u32[]{:S(2)}, u32[]{:S(2)}) %collective-permute-start.8) | collective-permute-done | bytes 1048608 | tf_op jit(solution)/shard_map/ppermute | solution.py:19
  529.9 43.6 %collective-permute-done.13 = bf16[1024,512]{1,0:T(8,128)(2,1)S(1)} collective-permute-done((bf16[1024,512]{1,0:T(8,128)(2,1)S(1)}, bf16[1024,512]{1,0:T(8,128)(2,1)S(1)}, u32[]{:S(2)}, u32[]{:S(2)}) %collective-permute-start.13) | collective-permute-done | bytes 1048608 | tf_op jit(solution)/shard_map/ppermute | solution.py:19
  575.0 18.0 %multiply_reduce_fusion.56 = (f32[8,512,8]{1,0,2:T(8,128)S(1)}, f32[8,512,8]{1,0,2:T(8,128)S(1)}, f32[8,512,8]{1,0,2:T(8,128)S(1)}, f32[8,512,8]{1,0,2:T(8,128)S...) fusion(bf16[8,8,64,512]{3,2,1,0:T(8,128)(2,1)S(1)} %bitcast.157, ...), kind=kLoop, calls=%fused_computation.134 | loop fusion | flops 117178368 | bytes 6356992 | tf_op jit(solution)/shard_map/hdc,shdc->shc/dot_general | solution.py:72
  593.8 20.8 %multiply_reduce_fusion.48 = (f32[8,512,8]{1,0,2:T(8,128)S(1)}, f32[8,512,8]{1,0,2:T(8,128)S(1)}, f32[8,512,8]{1,0,2:T(8,128)S(1)}, f32[8,512,8]{1,0,2:T(8,128)S...) fusion(bf16[8,8,64,7]{3,2,1,0:T(8,128)(2,1)S(1)} %slice.1097, ...), kind=kLoop, calls=%fused_computation.126 | loop fusion | flops 108789760 | bytes 10543104 | tf_op jit(solution)/shard_map/hdc,shdc->shc/dot_general | solution.py:72
  618.8 2.0 multiply_reduce_fusion.39
  620.9 9.1 multiply_reduce_fusion.41
  630.0 15.6 %multiply_reduce_fusion.46 = (f32[8,512,64]{1,2,0:T(8,128)}, f32[8,512,64]{1,2,0:T(8,128)}, f32[8,512,64]{1,2,0:T(8,128)}, f32[8,512,64]{1,2,0:T(8,128)}, f32[8,512,64]{1,2,0:T(8,128)}, /*index=5*/f32[8,512,64]{1,2,0:T(8,128)}) fusion(bf16[8,8,64,512]{3,2,1,0:T(8,128)(2,1)S(1)} %bitcast.1558, bf16[8,8,64,8]{3,2,1,0:T(8,128)(2,1)S(1)} %slice.1069, ...), kind=kLoop, calls=%fused_computation.124 | loop fusion | flops 86507520 | bytes 11337728 | tf_op jit(solution)/shard_map/shc,shdc->hdc/dot_general | solution.py:86
  645.6 18.8 %multiply_reduce_fusion.38 = (f32[8,512,64]{1,2,0:T(8,128)}, f32[8,512,64]{1,2,0:T(8,128)}, f32[8,512,64]{1,2,0:T(8,128)}, f32[8,512,64]{1,2,0:T(8,128)}, f32[8,512,64]{1,2,0:T(8,128)}, /*index=5*/f32[8,512,64]{1,2,0:T(8,128)}) fusion(bf16[8,8,64,512]{3,2,1,0:T(8,128)(2,1)S(1)} %bitcast.1559, bf16[8,8,64,7]{3,2,1,0:T(8,128)(2,1)S(1)} %slice.1138, ...), kind=kLoop, calls=%fused_computation.116 | loop fusion | flops 86507520 | bytes 11329536 | tf_op jit(solution)/shard_map/shc,shdc->hdc/dot_general | solution.py:86
  664.4 6.4 add_convert_fusion.1
  670.8 4.3 fusion.194
  675.2 30.4 %reduce-scatter.6.cloned.1.call-done = bf16[512,512]{0,1:T(8,128)(2,1)} async-done(((bf16[2048,512]{0,1:T(8,128)(2,1)}), bf16[512,512]{0,1:T(8,128)(2,1)}) %reduce-scatter.6.cloned.1.call-update) | async-done | bytes 524304 | tf_op jit(solution)/shard_map/reduce_scatter | solution.py:91
  705.6 2.0 add_convert_fusion.4
  707.6 22.7 %all-gather.10.cloned.1.call-done = bf16[2048,512]{0,1:T(8,128)(2,1)} async-done(((bf16[512,512]{0,1:T(8,128)(2,1)}), bf16[2048,512]{0,1:T(8,128)(2,1)}) %all-gather.10.cloned.1.call-update) | async-done | bytes 2097168 | tf_op jit(solution)/shard_map/all_gather | solution.py:41
  730.3 2.1 fusion.165
  732.4 5.6 multiply_convert_fusion
  738.0 2.4 collective-permute-start.14
  740.4 2.4 collective-permute-start.15
  745.1 3.7 collective-permute-start.18
  748.8 3.5 bitcast_convert_fusion
  752.3 80.2 %collective-permute-done.14 = bf16[1024,512]{1,0:T(8,128)(2,1)S(1)} collective-permute-done((bf16[1024,512]{1,0:T(8,128)(2,1)}, bf16[1024,512]{1,0:T(8,128)(2,1)S(1)}, u32[]{:S(2)}, u32[]{:S(2)}) %collective-permute-start.14) | collective-permute-done | bytes 1048608 | tf_op jit(solution)/shard_map/ppermute | solution.py:19
  832.6 45.8 %collective-permute-done.15 = bf16[1024,512]{1,0:T(8,128)(2,1)S(1)} collective-permute-done((bf16[1024,512]{1,0:T(8,128)(2,1)}, bf16[1024,512]{1,0:T(8,128)(2,1)S(1)}, u32[]{:S(2)}, u32[]{:S(2)}) %collective-permute-start.15) | collective-permute-done | bytes 1048608 | tf_op jit(solution)/shard_map/ppermute | solution.py:19
  878.7 1.3 bitcast_dynamic-update-slice_fusion.3
  880.1 42.4 %collective-permute-done.20 = bf16[1024,512]{1,0:T(8,128)(2,1)S(1)} collective-permute-done((bf16[1024,512]{1,0:T(8,128)(2,1)}, bf16[1024,512]{1,0:T(8,128)(2,1)S(1)}, u32[]{:S(2)}, u32[]{:S(2)}) %collective-permute-start.20) | collective-permute-done | bytes 1048608 | tf_op jit(solution)/shard_map/ppermute | solution.py:19
  924.3 18.0 %multiply_reduce_fusion.24 = (f32[8,512,8]{1,0,2:T(8,128)S(1)}, f32[8,512,8]{1,0,2:T(8,128)S(1)}, f32[8,512,8]{1,0,2:T(8,128)S(1)}, f32[8,512,8]{1,0,2:T(8,128)S...) fusion(bf16[8,8,64,512]{3,2,1,0:T(8,128)(2,1)S(1)} %bitcast.157, ...), kind=kLoop, calls=%fused_computation.102 | loop fusion | flops 117178368 | bytes 6356992 | tf_op jit(solution)/shard_map/hdc,shdc->shc/dot_general | solution.py:72
  943.0 20.8 %multiply_reduce_fusion.16 = (f32[8,512,8]{1,0,2:T(8,128)S(1)}, f32[8,512,8]{1,0,2:T(8,128)S(1)}, f32[8,512,8]{1,0,2:T(8,128)S(1)}, f32[8,512,8]{1,0,2:T(8,128)S...) fusion(bf16[8,8,64,7]{3,2,1,0:T(8,128)(2,1)S(1)} %slice.1187, ...), kind=kLoop, calls=%fused_computation.94 | loop fusion | flops 108789760 | bytes 10543104 | tf_op jit(solution)/shard_map/hdc,shdc->shc/dot_general | solution.py:72
  968.1 2.1 multiply_reduce_fusion.7
  970.1 9.0 multiply_reduce_fusion.9
  979.2 15.6 %multiply_reduce_fusion.14 = (f32[8,512,64]{1,2,0:T(8,128)}, f32[8,512,64]{1,2,0:T(8,128)}, f32[8,512,64]{1,2,0:T(8,128)}, f32[8,512,64]{1,2,0:T(8,128)}, f32[8,512,64]{1,2,0:T(8,128)}, /*index=5*/f32[8,512,64]{1,2,0:T(8,128)}) fusion(bf16[8,8,64,512]{3,2,1,0:T(8,128)(2,1)S(1)} %bitcast.1564, bf16[8,8,64,8]{3,2,1,0:T(8,128)(2,1)S(1)} %slice.1159, ...), kind=kLoop, calls=%fused_computation.92 | loop fusion | flops 86507520 | bytes 11337728 | tf_op jit(solution)/shard_map/shc,shdc->hdc/dot_general | solution.py:86
  994.8 18.8 %multiply_reduce_fusion.6 = (f32[8,512,64]{1,2,0:T(8,128)}, f32[8,512,64]{1,2,0:T(8,128)}, f32[8,512,64]{1,2,0:T(8,128)}, f32[8,512,64]{1,2,0:T(8,128)}, f32[8,512,64]{1,2,0:T(8,128)}, /*index=5*/f32[8,512,64]{1,2,0:T(8,128)}) fusion(bf16[8,8,64,512]{3,2,1,0:T(8,128)(2,1)S(1)} %bitcast.1565, bf16[8,8,64,7]{3,2,1,0:T(8,128)(2,1)S(1)} %slice.1228, ...), kind=kLoop, calls=%fused_computation.84 | loop fusion | flops 86507520 | bytes 11329536 | tf_op jit(solution)/shard_map/shc,shdc->hdc/dot_general | solution.py:86
  1013.6 6.4 add_convert_fusion
  1020.0 4.3 fusion.195
  1024.3 31.1 %reduce-scatter.8.cloned.1.call-done = bf16[512,512]{0,1:T(8,128)(2,1)} async-done(((bf16[2048,512]{0,1:T(8,128)(2,1)}), bf16[512,512]{0,1:T(8,128)(2,1)}) %reduce-scatter.8.cloned.1.call-update) | async-done | bytes 524304 | tf_op jit(solution)/shard_map/reduce_scatter | solution.py:91
  (281 shorter events, 31.7 us)
Async XLA Ops:
  6.5 27.7 %all-gather.6.cloned.1.call-start = ((), (), s32[]{:S(2)}) async-start(), calls=%async_computation.3 | async-start | bytes 2621440 | tf_op jit(solution)/shard_map/all_gather | solution.py:41
  7.3 350.4 %reduce-scatter.4.cloned.1.call-start = ((), (), s32[]{:S(2)}) async-start(), calls=%async_computation.4 | async-start | bytes 2621440 | tf_op jit(solution)/shard_map/reduce_scatter | solution.py:91
  36.3 9.5 copy-start.18
  41.0 94.6 %collective-permute-start = (bf16[1024,512]{1,0:T(8,128)(2,1)S(1)}, bf16[1024,512]{1,0:T(8,128)(2,1)}, u32[]{:S(2)}, u32[]{:S(2)}) collective-permute-start(bf16[1024,512]{1,0:T(8,128)(2,1)S(1)} %multiply_convert_fusion.2), channel_id=1, source_target_pairs={{16,0},{20,4},{24,8},{28,12},{0,16},{4,20},{8,24},{12,28},{17,1},{... | collective-permute-start | bytes 3145736 | tf_op jit(solution)/shard_map/ppermute | solution.py:19
  43.5 137.8 %collective-permute-start.1 = (bf16[1024,512]{1,0:T(8,128)(2,1)S(1)}, bf16[1024,512]{1,0:T(8,128)(2,1)S(1)}, u32[]{:S(2)}, u32[]{:S(2)}) collective-permute-start(bf16[1024,512]{1,0:T(8,128)(2,1)S(1)} %multiply_convert_fusion.2), channel_id=1, source_target_pairs={{20,0},{24,4},{28,8},{0,12},{4,16},{8,20},{12,24},{16,28},{21,1},{... | collective-permute-start | bytes 3145736 | tf_op jit(solution)/shard_map/ppermute | solution.py:19
  46.6 135.1 %collective-permute-start.2 = (bf16[1024,512]{1,0:T(8,128)(2,1)S(1)}, bf16[1024,512]{1,0:T(8,128)(2,1)S(1)}, u32[]{:S(2)}, u32[]{:S(2)}) collective-permute-start(bf16[1024,512]{1,0:T(8,128)(2,1)S(1)} %multiply_convert_fusion.2), channel_id=1, source_target_pairs={{24,0},{28,4},{0,8},{4,12},{8,16},{12,20},{16,24},{20,28},{25,1},{... | collective-permute-start | bytes 3145736 | tf_op jit(solution)/shard_map/ppermute | solution.py:19
  47.8 134.0 %collective-permute-start.3 = (bf16[1024,512]{1,0:T(8,128)(2,1)S(1)}, bf16[1024,512]{1,0:T(8,128)(2,1)S(1)}, u32[]{:S(2)}, u32[]{:S(2)}) collective-permute-start(bf16[1024,512]{1,0:T(8,128)(2,1)S(1)} %multiply_convert_fusion.2), channel_id=1, source_target_pairs={{28,0},{0,4},{4,8},{8,12},{12,16},{16,20},{20,24},{24,28},{29,1},{... | collective-permute-start | bytes 3145736 | tf_op jit(solution)/shard_map/ppermute | solution.py:19
  48.8 133.1 %collective-permute-start.4 = (bf16[1024,512]{1,0:T(8,128)(2,1)S(1)}, bf16[1024,512]{1,0:T(8,128)(2,1)S(1)}, u32[]{:S(2)}, u32[]{:S(2)}) collective-permute-start(bf16[1024,512]{1,0:T(8,128)(2,1)S(1)} %multiply_convert_fusion.2), channel_id=1, source_target_pairs={{4,0},{8,4},{12,8},{16,12},{20,16},{24,20},{28,24},{0,28},{5,1},{9... | collective-permute-start | bytes 3145736 | tf_op jit(solution)/shard_map/ppermute | solution.py:19
  135.6 46.4 %collective-permute-start.5 = (bf16[1024,512]{1,0:T(8,128)(2,1)S(1)}, bf16[1024,512]{1,0:T(8,128)(2,1)S(1)}, u32[]{:S(2)}, u32[]{:S(2)}) collective-permute-start(bf16[1024,512]{1,0:T(8,128)(2,1)S(1)} %multiply_convert_fusion.2), channel_id=1, source_target_pairs={{8,0},{12,4},{16,8},{20,12},{24,16},{28,20},{0,24},{4,28},{9,1},{1... | collective-permute-start | bytes 3145736 | tf_op jit(solution)/shard_map/ppermute | solution.py:19
  181.3 44.2 %collective-permute-start.6 = (bf16[1024,512]{1,0:T(8,128)(2,1)S(1)}, bf16[1024,512]{1,0:T(8,128)(2,1)S(1)}, u32[]{:S(2)}, u32[]{:S(2)}) collective-permute-start(bf16[1024,512]{1,0:T(8,128)(2,1)S(1)} %multiply_convert_fusion.2), channel_id=1, source_target_pairs={{12,0},{16,4},{20,8},{24,12},{28,16},{0,20},{4,24},{8,28},{13,1},{... | collective-permute-start | bytes 3145736 | tf_op jit(solution)/shard_map/ppermute | solution.py:19
  297.3 19.1 %copy-start.2 = (f32[8,512,64]{1,2,0:T(8,128)S(1)}, f32[8,512,64]{1,2,0:T(8,128)}, u32[]{:S(2)}) copy-start(f32[8,512,64]{1,2,0:T(8,128)} %get-tuple-element.84) | copy-start | bytes 3145732
  297.3 19.1 %copy-start.3 = (f32[8,512,64]{1,2,0:T(8,128)S(1)}, f32[8,512,64]{1,2,0:T(8,128)}, u32[]{:S(2)}) copy-start(f32[8,512,64]{1,2,0:T(8,128)} %get-tuple-element.85) | copy-start | bytes 3145732
  297.3 19.1 %copy-start.4 = (f32[8,512,64]{1,2,0:T(8,128)S(1)}, f32[8,512,64]{1,2,0:T(8,128)}, u32[]{:S(2)}) copy-start(f32[8,512,64]{1,2,0:T(8,128)} %get-tuple-element.94) | copy-start | bytes 3145732
  297.3 19.1 %copy-start.11 = (f32[8,512,64]{1,2,0:T(8,128)S(1)}, f32[8,512,64]{1,2,0:T(8,128)}, u32[]{:S(2)}) copy-start(f32[8,512,64]{1,2,0:T(8,128)} %get-tuple-element.78) | copy-start | bytes 3145732
  322.9 4.4 copy-start.16
  327.2 57.3 %copy-start.15 = (bf16[2048,512]{1,0:T(8,128)(2,1)S(1)}, bf16[2048,512]{1,0:T(8,128)(2,1)}, u32[]{:S(2)}) copy-start(bf16[2048,512]{1,0:T(8,128)(2,1)} %get-tuple-element.109) | copy-start | bytes 6291460
  327.2 57.3 %copy-start.19 = (f32[1,2048]{1,0:T(1,128)S(1)}, f32[1,2048]{1,0:T(1,128)}, u32[]{:S(2)}) copy-start(f32[1,2048]{1,0:T(1,128)} %get-tuple-element.211) | copy-start | bytes 24580
  327.2 55.2 %all-gather.8.cloned.1.call-start = ((), (), s32[]{:S(2)}) async-start(), calls=%async_computation.7 | async-start | bytes 2621440 | tf_op jit(solution)/shard_map/all_gather | solution.py:41
  359.7 345.9 %reduce-scatter.6.cloned.1.call-start = ((), (), s32[]{:S(2)}) async-start(), calls=%async_computation.5 | async-start | bytes 2621440 | tf_op jit(solution)/shard_map/reduce_scatter | solution.py:91
  384.5 9.5 copy-start.17
  389.1 94.6 %collective-permute-start.7 = (bf16[1024,512]{1,0:T(8,128)(2,1)S(1)}, bf16[1024,512]{1,0:T(8,128)(2,1)}, u32[]{:S(2)}, u32[]{:S(2)}) collective-permute-start(bf16[1024,512]{1,0:T(8,128)(2,1)S(1)} %multiply_convert_fusion.1), channel_id=1, source_target_pairs={{16,0},{20,4},{24,8},{28,12},{0,16},{4,20},{8,24},{12,28},{17,1},{... | collective-permute-start | bytes 3145736 | tf_op jit(solution)/shard_map/ppermute | solution.py:19
  391.6 137.8 %collective-permute-start.8 = (bf16[1024,512]{1,0:T(8,128)(2,1)S(1)}, bf16[1024,512]{1,0:T(8,128)(2,1)S(1)}, u32[]{:S(2)}, u32[]{:S(2)}) collective-permute-start(bf16[1024,512]{1,0:T(8,128)(2,1)S(1)} %multiply_convert_fusion.1), channel_id=1, source_target_pairs={{20,0},{24,4},{28,8},{0,12},{4,16},{8,20},{12,24},{16,28},{21,1},{... | collective-permute-start | bytes 3145736 | tf_op jit(solution)/shard_map/ppermute | solution.py:19
  394.1 135.4 %collective-permute-start.9 = (bf16[1024,512]{1,0:T(8,128)(2,1)S(1)}, bf16[1024,512]{1,0:T(8,128)(2,1)S(1)}, u32[]{:S(2)}, u32[]{:S(2)}) collective-permute-start(bf16[1024,512]{1,0:T(8,128)(2,1)S(1)} %multiply_convert_fusion.1), channel_id=1, source_target_pairs={{24,0},{28,4},{0,8},{4,12},{8,16},{12,20},{16,24},{20,28},{25,1},{... | collective-permute-start | bytes 3145736 | tf_op jit(solution)/shard_map/ppermute | solution.py:19
  395.3 134.3 %collective-permute-start.10 = (bf16[1024,512]{1,0:T(8,128)(2,1)S(1)}, bf16[1024,512]{1,0:T(8,128)(2,1)S(1)}, u32[]{:S(2)}, u32[]{:S(2)}) collective-permute-start(bf16[1024,512]{1,0:T(8,128)(2,1)S(1)} %multiply_convert_fusion.1), channel_id=1, source_target_pairs={{28,0},{0,4},{4,8},{8,12},{12,16},{16,20},{20,24},{24,28},{29,1},{... | collective-permute-start | bytes 3145736 | tf_op jit(solution)/shard_map/ppermute | solution.py:19
  396.3 133.4 %collective-permute-start.11 = (bf16[1024,512]{1,0:T(8,128)(2,1)S(1)}, bf16[1024,512]{1,0:T(8,128)(2,1)S(1)}, u32[]{:S(2)}, u32[]{:S(2)}) collective-permute-start(bf16[1024,512]{1,0:T(8,128)(2,1)S(1)} %multiply_convert_fusion.1), channel_id=1, source_target_pairs={{4,0},{8,4},{12,8},{16,12},{20,16},{24,20},{28,24},{0,28},{5,1},{9... | collective-permute-start | bytes 3145736 | tf_op jit(solution)/shard_map/ppermute | solution.py:19
  483.7 46.2 %collective-permute-start.12 = (bf16[1024,512]{1,0:T(8,128)(2,1)S(1)}, bf16[1024,512]{1,0:T(8,128)(2,1)S(1)}, u32[]{:S(2)}, u32[]{:S(2)}) collective-permute-start(bf16[1024,512]{1,0:T(8,128)(2,1)S(1)} %multiply_convert_fusion.1), channel_id=1, source_target_pairs={{8,0},{12,4},{16,8},{20,12},{24,16},{28,20},{0,24},{4,28},{9,1},{1... | collective-permute-start | bytes 3145736 | tf_op jit(solution)/shard_map/ppermute | solution.py:19
  529.4 44.2 %collective-permute-start.13 = (bf16[1024,512]{1,0:T(8,128)(2,1)S(1)}, bf16[1024,512]{1,0:T(8,128)(2,1)S(1)}, u32[]{:S(2)}, u32[]{:S(2)}) collective-permute-start(bf16[1024,512]{1,0:T(8,128)(2,1)S(1)} %multiply_convert_fusion.1), channel_id=1, source_target_pairs={{12,0},{16,4},{20,8},{24,12},{28,16},{0,20},{4,24},{8,28},{13,1},{... | collective-permute-start | bytes 3145736 | tf_op jit(solution)/shard_map/ppermute | solution.py:19
  645.6 18.8 %copy-start.5 = (f32[8,512,64]{1,2,0:T(8,128)S(1)}, f32[8,512,64]{1,2,0:T(8,128)}, u32[]{:S(2)}) copy-start(f32[8,512,64]{1,2,0:T(8,128)} %get-tuple-element.70) | copy-start | bytes 3145732
  645.6 18.8 %copy-start.6 = (f32[8,512,64]{1,2,0:T(8,128)S(1)}, f32[8,512,64]{1,2,0:T(8,128)}, u32[]{:S(2)}) copy-start(f32[8,512,64]{1,2,0:T(8,128)} %get-tuple-element.71) | copy-start | bytes 3145732
  645.6 18.8 %copy-start.7 = (f32[8,512,64]{1,2,0:T(8,128)S(1)}, f32[8,512,64]{1,2,0:T(8,128)}, u32[]{:S(2)}) copy-start(f32[8,512,64]{1,2,0:T(8,128)} %get-tuple-element.93) | copy-start | bytes 3145732
  645.6 18.8 %copy-start.12 = (f32[8,512,64]{1,2,0:T(8,128)S(1)}, f32[8,512,64]{1,2,0:T(8,128)}, u32[]{:S(2)}) copy-start(f32[8,512,64]{1,2,0:T(8,128)} %get-tuple-element.64) | copy-start | bytes 3145732
  670.8 34.7 %copy-start.1 = (bf16[512,512]{0,1:T(8,128)(2,1)S(1)}, bf16[512,512]{0,1:T(8,128)(2,1)}, u32[]{:S(2)}) copy-start(bf16[512,512]{0,1:T(8,128)(2,1)} %fusion.271) | copy-start | bytes 1572868
  675.1 57.3 %copy-start.14 = (bf16[2048,512]{1,0:T(8,128)(2,1)S(1)}, bf16[2048,512]{1,0:T(8,128)(2,1)}, u32[]{:S(2)}) copy-start(bf16[2048,512]{1,0:T(8,128)(2,1)} %get-tuple-element.107) | copy-start | bytes 6291460
  675.1 55.2 %all-gather.10.cloned.1.call-start = ((), (), s32[]{:S(2)}) async-start(), calls=%async_computation.8 | async-start | bytes 2621440 | tf_op jit(solution)/shard_map/all_gather | solution.py:41
  707.6 347.8 %reduce-scatter.8.cloned.1.call-start = ((), (), s32[]{:S(2)}) async-start(), calls=%async_computation.6 | async-start | bytes 2621440 | tf_op jit(solution)/shard_map/reduce_scatter | solution.py:91
  738.0 94.6 %collective-permute-start.14 = (bf16[1024,512]{1,0:T(8,128)(2,1)}, bf16[1024,512]{1,0:T(8,128)(2,1)S(1)}, u32[]{:S(2)}, u32[]{:S(2)}) collective-permute-start(bf16[1024,512]{1,0:T(8,128)(2,1)} %multiply_convert_fusion), channel_id=1, source_target_pairs={{16,0},{20,4},{24,8},{28,12},{0,16},{4,20},{8,24},{12,28},{17,1},{... | collective-permute-start | bytes 3145736 | tf_op jit(solution)/shard_map/ppermute | solution.py:19
  740.4 138.0 %collective-permute-start.15 = (bf16[1024,512]{1,0:T(8,128)(2,1)}, bf16[1024,512]{1,0:T(8,128)(2,1)S(1)}, u32[]{:S(2)}, u32[]{:S(2)}) collective-permute-start(bf16[1024,512]{1,0:T(8,128)(2,1)} %multiply_convert_fusion), channel_id=1, source_target_pairs={{20,0},{24,4},{28,8},{0,12},{4,16},{8,20},{12,24},{16,28},{21,1},{... | collective-permute-start | bytes 3145736 | tf_op jit(solution)/shard_map/ppermute | solution.py:19
  742.9 135.6 %collective-permute-start.16 = (bf16[1024,512]{1,0:T(8,128)(2,1)}, bf16[1024,512]{1,0:T(8,128)(2,1)S(1)}, u32[]{:S(2)}, u32[]{:S(2)}) collective-permute-start(bf16[1024,512]{1,0:T(8,128)(2,1)} %multiply_convert_fusion), channel_id=1, source_target_pairs={{24,0},{28,4},{0,8},{4,12},{8,16},{12,20},{16,24},{20,28},{25,1},{... | collective-permute-start | bytes 3145736 | tf_op jit(solution)/shard_map/ppermute | solution.py:19
  744.0 134.5 %collective-permute-start.17 = (bf16[1024,512]{1,0:T(8,128)(2,1)}, bf16[1024,512]{1,0:T(8,128)(2,1)S(1)}, u32[]{:S(2)}, u32[]{:S(2)}) collective-permute-start(bf16[1024,512]{1,0:T(8,128)(2,1)} %multiply_convert_fusion), channel_id=1, source_target_pairs={{28,0},{0,4},{4,8},{8,12},{12,16},{16,20},{20,24},{24,28},{29,1},{... | collective-permute-start | bytes 3145736 | tf_op jit(solution)/shard_map/ppermute | solution.py:19
  745.1 134.9 %collective-permute-start.18 = (bf16[1024,512]{1,0:T(8,128)(2,1)}, bf16[1024,512]{1,0:T(8,128)(2,1)S(1)}, u32[]{:S(2)}, u32[]{:S(2)}) collective-permute-start(bf16[1024,512]{1,0:T(8,128)(2,1)} %multiply_convert_fusion), channel_id=1, source_target_pairs={{4,0},{8,4},{12,8},{16,12},{20,16},{24,20},{28,24},{0,28},{5,1},{9... | collective-permute-start | bytes 3145736 | tf_op jit(solution)/shard_map/ppermute | solution.py:19
  832.6 47.5 %collective-permute-start.19 = (bf16[1024,512]{1,0:T(8,128)(2,1)}, bf16[1024,512]{1,0:T(8,128)(2,1)S(1)}, u32[]{:S(2)}, u32[]{:S(2)}) collective-permute-start(bf16[1024,512]{1,0:T(8,128)(2,1)} %multiply_convert_fusion), channel_id=1, source_target_pairs={{8,0},{12,4},{16,8},{20,12},{24,16},{28,20},{0,24},{4,28},{9,1},{1... | collective-permute-start | bytes 3145736 | tf_op jit(solution)/shard_map/ppermute | solution.py:19
  878.4 44.2 %collective-permute-start.20 = (bf16[1024,512]{1,0:T(8,128)(2,1)}, bf16[1024,512]{1,0:T(8,128)(2,1)S(1)}, u32[]{:S(2)}, u32[]{:S(2)}) collective-permute-start(bf16[1024,512]{1,0:T(8,128)(2,1)} %multiply_convert_fusion), channel_id=1, source_target_pairs={{12,0},{16,4},{20,8},{24,12},{28,16},{0,20},{4,24},{8,28},{13,1},{... | collective-permute-start | bytes 3145736 | tf_op jit(solution)/shard_map/ppermute | solution.py:19
  994.8 18.8 %copy-start.8 = (f32[8,512,64]{1,2,0:T(8,128)S(1)}, f32[8,512,64]{1,2,0:T(8,128)}, u32[]{:S(2)}) copy-start(f32[8,512,64]{1,2,0:T(8,128)} %get-tuple-element.56) | copy-start | bytes 3145732
  994.8 18.8 %copy-start.9 = (f32[8,512,64]{1,2,0:T(8,128)S(1)}, f32[8,512,64]{1,2,0:T(8,128)}, u32[]{:S(2)}) copy-start(f32[8,512,64]{1,2,0:T(8,128)} %get-tuple-element.57) | copy-start | bytes 3145732
  994.8 18.8 %copy-start.10 = (f32[8,512,64]{1,2,0:T(8,128)S(1)}, f32[8,512,64]{1,2,0:T(8,128)}, u32[]{:S(2)}) copy-start(f32[8,512,64]{1,2,0:T(8,128)} %get-tuple-element.92) | copy-start | bytes 3145732
  994.8 18.8 %copy-start.13 = (f32[8,512,64]{1,2,0:T(8,128)S(1)}, f32[8,512,64]{1,2,0:T(8,128)}, u32[]{:S(2)}) copy-start(f32[8,512,64]{1,2,0:T(8,128)} %get-tuple-element.50) | copy-start | bytes 3145732
  1020.0 35.4 %copy-start = (bf16[512,512]{0,1:T(8,128)(2,1)S(1)}, bf16[512,512]{0,1:T(8,128)(2,1)}, u32[]{:S(2)}) copy-start(bf16[512,512]{0,1:T(8,128)(2,1)} %add_convert_fusion.4) | copy-start | bytes 1572868
Sparse Core Ops, SparseCore 0:
  8.9 25.2 all-gather.5
  327.4 30.2 reduce-scatter.3
  359.8 22.5 all-gather.7
  675.2 30.2 reduce-scatter.5
  707.7 22.5 all-gather.9
  1024.4 30.9 reduce-scatter.7
where the time goes:
time: 1070 us; the launch traced here: 1060 us
  waiting for transfers between devices  658 us (61%)
  other arithmetic  298 us (28%)
  matrix products  38.5 us (4%)
  starting transfers between devices  29.4 us (3%)
  local copies, waits for them, and re-layouts  25.7 us (2%)
  between operations  14.7 us (1%)
    ppermute x21, waiting for transfers between devices, from_behind(): return lax.ppermute(block, axis, route)  504 us
    dot_general x12, other arithmetic, body(): jnp.einsum('shc,shdc->hdc', weights[offset], shifted, preferred_element_t...  137 us
    dot_general x6, other arithmetic, body(): jnp.einsum('hdc,shdc->shc', query_heads, shifted, preferred_element_type=...  116 us
    reduce_scatter x3, waiting for transfers between devices, body(): lax.psum_scatter(lax.dot_general(w_layer, mixed_out, (((0,), (0,)), ((),...  91.6 us
    all_gather x3, waiting for transfers between devices, body(): lax.all_gather(current, 'tp', axis=1, tiled=True)[0].astype(jnp.float32)  61.9 us
    ppermute x21, starting transfers between devices, from_behind(): return lax.ppermute(block, axis, route)  29.2 us
  transfers between devices with their start and end apart: 27, of which 15 were waited for; matrix products, arithmetic and copies ran while one was open for 3% of the time, Pallas kernels for 0%

commit v1 on v0

v1 whole, which is shorter than its diff:
```python
import functools

import jax
import jax.numpy as jnp
from jax import lax
from jax.experimental import pallas as pl
from jax.experimental.pallas import tpu as pltpu
from jax.sharding import PartitionSpec as P

HEAD_DIM = 64
WIN_R = 8
WIN_C = 16
EPS = 1e-06
LANES = 128
NEG = -1e30


def attention_kernel(rows, cols, q_ref, k_ref, v_ref, kh_ref, vh_ref, base_ref, o_ref, tile_ref):
    pack = LANES // cols
    n_slots = min(rows, pack + WIN_R - 1)
    half_r = WIN_R // 2
    span = cols + WIN_C
    lane = lax.broadcasted_iota(jnp.int32, (8, LANES), 1)
    lane_q = lax.broadcasted_iota(jnp.int32, (LANES, LANES), 1)
    v_main = v_ref[...].T
    v_halo = vh_ref[...].T
    neg = jnp.full((8, LANES), NEG, jnp.float32)
    outs = [[] for _ in range(rows * cols // LANES)]
    for head in range(LANES // HEAD_DIM):
        for p in range(pack):
            own = (lane >= p * cols) & (lane < (p + 1) * cols)
            for slot in range(WIN_R):
                e = (slot + p) % rows
                start = jnp.broadcast_to(base_ref[head, slot : slot + 1, :], (8, LANES))
                start = pltpu.roll(start, 0, 1, stride=1, stride_axis=0)
                for blk in range(span // 8):
                    shift = (p * cols + 8 * blk) % LANES
                    moved = pltpu.roll(start, shift, 1) if shift else start
                    at = blk - 1 if 1 <= blk <= cols // 8 else (cols // 8 if blk == 0 else blk)
                    where = pl.ds(e * span + 8 * at, 8)
                    rest = neg if p == 0 and rows == WIN_R else tile_ref[where, :]
                    tile_ref[where, :] = jnp.where(own, moved, rest)
        for group in range(rows * cols // LANES):
            key_rows = [r for r in range(rows) if (r - group * pack + half_r) % rows < n_slots]
            q = q_ref[group * LANES : (group + 1) * LANES, :]
            mine = (lane_q >= head * HEAD_DIM) & (lane_q < (head + 1) * HEAD_DIM)
            q = jnp.where(mine, q, jnp.zeros_like(q))
            s_list = []
            contract = (((1,), (1,)), ((), ()))
            if len(key_rows) == rows:
                s_main = lax.dot_general(k_ref[...], q, contract, preferred_element_type=jnp.float32)
                s_halo = lax.dot_general(kh_ref[...], q, contract, preferred_element_type=jnp.float32)
            main_list = []
            halo_list = []
            for r in key_rows:
                e = (r - group * pack + half_r) % rows
                if len(key_rows) == rows:
                    main = s_main[r * cols : (r + 1) * cols]
                    halo = s_halo[r * WIN_C : (r + 1) * WIN_C]
                else:
                    main = lax.dot_general(
                        k_ref[r * cols : (r + 1) * cols, :], q, contract, preferred_element_type=jnp.float32
                    )
                    halo = lax.dot_general(
                        kh_ref[r * WIN_C : (r + 1) * WIN_C, :], q, contract, preferred_element_type=jnp.float32
                    )
                main_list.append(main + tile_ref[e * span : e * span + cols, :])
                halo_list.append(halo + tile_ref[e * span + cols : (e + 1) * span, :])
            main = jnp.concatenate(main_list, axis=0)
            halo = jnp.concatenate(halo_list, axis=0)
            top = jnp.maximum(jnp.max(main, axis=0, keepdims=True), jnp.max(halo, axis=0, keepdims=True))
            main = jnp.exp(main - top)
            halo = jnp.exp(halo - top)
            total = jnp.sum(main, axis=0, keepdims=True) + jnp.sum(halo, axis=0, keepdims=True)
            main = main.astype(jnp.bfloat16)
            halo = halo.astype(jnp.bfloat16)
            lo = head * HEAD_DIM
            if len(key_rows) == rows:
                vm = v_main[lo : lo + HEAD_DIM]
                vh = v_halo[lo : lo + HEAD_DIM]
            else:
                vm = jnp.concatenate([v_main[lo : lo + HEAD_DIM, r * cols : (r + 1) * cols] for r in key_rows], axis=1)
                vh = jnp.concatenate(
                    [v_halo[lo : lo + HEAD_DIM, r * WIN_C : (r + 1) * WIN_C] for r in key_rows], axis=1
                )
            mixed = jnp.dot(vm, main, preferred_element_type=jnp.float32)
            mixed = mixed + jnp.dot(vh, halo, preferred_element_type=jnp.float32)
            outs[group].append(mixed / total)
    for group in range(rows * cols // LANES):
        both = jnp.concatenate(outs[group], axis=0)
        o_ref[group * LANES : (group + 1) * LANES, :] = both.T.astype(o_ref.dtype)


def attention_kernel_init(rows, cols, *refs):
    tile_ref = refs[-1]
    tile_ref[...] = jnp.full(tile_ref.shape, NEG, jnp.float32)
    attention_kernel(rows, cols, *refs)


def attention(queries, keys, values, halo, base, rows, cols):
    tokens, channels = queries.shape
    n_slots = min(rows, LANES // cols + WIN_R - 1)
    pairs = channels // LANES
    per = LANES // HEAD_DIM
    side = halo.shape[0]
    kernel = attention_kernel if rows == WIN_R else attention_kernel_init
    return pl.pallas_call(
        functools.partial(kernel, rows, cols),
        grid=(pairs,),
        out_shape=jax.ShapeDtypeStruct((tokens, channels), jnp.bfloat16),
        in_specs=[
            pl.BlockSpec((tokens, LANES), lambda i: (0, i)),
            pl.BlockSpec((tokens, LANES), lambda i: (0, i)),
            pl.BlockSpec((tokens, LANES), lambda i: (0, i)),
            pl.BlockSpec((side, LANES), lambda i: (0, i)),
            pl.BlockSpec((side, LANES), lambda i: (0, i + pairs)),
            pl.BlockSpec((per, WIN_R, LANES), lambda i: (i, 0, 0)),
        ],
        out_specs=pl.BlockSpec((tokens, LANES), lambda i: (0, i)),
        scratch_shapes=[pltpu.VMEM((n_slots * (cols + WIN_C), LANES), jnp.float32)],
        compiler_params=pltpu.CompilerParams(vmem_limit_bytes=48 * 1024 * 1024),
        name="window_attention",
    )(queries, keys, values, halo, halo, base)


def body(token_grid, norm_gain, w_query, w_key, w_value, w_out, rel_bias):
    n = lax.axis_size("sp")
    rows_dev, channels, columns = token_grid.shape
    rows = rows_dev * n
    cols = columns // n
    tokens = rows * cols
    width = norm_gain.shape[1]
    factor = HEAD_DIM ** (-0.5)
    half_c = WIN_C // 2
    base = jnp.concatenate(
        [
            rel_bias[..., :1],
            jnp.full(rel_bias.shape[:-1] + (LANES - WIN_C,), NEG, jnp.float32),
            jnp.flip(rel_bias[..., 1:], axis=-1),
        ],
        axis=-1,
    )
    turned = jnp.transpose(token_grid, (2, 0, 1)).reshape(columns, rows_dev * channels)
    current = lax.all_to_all(turned, "sp", split_axis=0, concat_axis=0, tiled=True)
    to_right = [(i, (i + 1) % n) for i in range(n)]
    to_left = [(i, (i - 1) % n) for i in range(n)]
    for layer in range(norm_gain.shape[0]):
        gain = norm_gain[layer].astype(jnp.float32)
        raw = lax.all_gather(current, "tp", axis=1, tiled=True).astype(jnp.float32)
        scaled = (raw * gain[None, :]).astype(jnp.bfloat16)
        inverse = lax.rsqrt(jnp.sum(raw * raw, axis=1, keepdims=True) / width + EPS)

        def project(weight, scale=1.0):
            product = jnp.dot(scaled, weight[layer], preferred_element_type=jnp.float32)
            return (product * inverse).astype(jnp.bfloat16) * jnp.bfloat16(scale)

        keys = project(w_key)
        values = project(w_value)
        keyval = jnp.concatenate([keys, values], axis=1).reshape(rows, cols, 2 * channels)
        left = lax.ppermute(keyval[:, cols - half_c :], "sp", to_right)
        right = lax.ppermute(keyval[:, :half_c], "sp", to_left)
        queries = project(w_query, factor)
        halo = jnp.concatenate([left, right], axis=1).reshape(rows * WIN_C, 2 * channels)
        mixed = attention(queries, keys, values, halo, base[layer], rows, cols)
        partial = jnp.dot(mixed, w_out[layer], preferred_element_type=jnp.float32).astype(jnp.bfloat16)
        update = lax.psum_scatter(partial, "tp", scatter_dimension=1, tiled=True)
        current = (current.astype(jnp.float32) + update.astype(jnp.float32)).astype(jnp.bfloat16)
    back = lax.all_to_all(current, "sp", split_axis=0, concat_axis=0, tiled=True)
    return jnp.transpose(back.reshape(columns, rows_dev, channels), (1, 2, 0))


def solution(mesh):
    in_specs = (
        P("sp", "tp", None),
        P(),
        P(None, None, "tp"),
        P(None, None, "tp"),
        P(None, None, "tp"),
        P(None, "tp", None),
        P(None, "tp", None, None),
    )
    out_specs = P("sp", "tp", None)
    return jax.shard_map(body, mesh=mesh, in_specs=in_specs, out_specs=out_specs, check_vma=False)
```

time: 1070 us -> 321 us (0.30)
  waiting for transfers between devices: 658 us -> 165 us
  other arithmetic: 298 us -> 12.4 us
  blocking collectives: 0 us -> 41.4 us
  Pallas kernels: 0 us -> 33.8 us
  local copies, waits for them, and re-layouts: 25.7 us -> 2.64 us
  starting transfers between devices: 29.4 us -> 13.1 us
    ppermute x21 -> x6, waiting for transfers between devices: 504 us -> 15.6 us  [the longest x3 14.7 us: body(): left = lax.ppermute(keyval[:, cols - half_c:], 'sp', to_right)]
    dot_general x18 -> x0, other arithmetic: 253 us -> none  [the longest x12 137 us: body(): jnp.einsum('shc,shdc->hdc', weights[offset], shifted, preferred_element_t...]
    all_to_all x0 -> x2, blocking collectives: none -> 41.4 us  [the longest x1 21.7 us: body(): lax.all_to_all(turned, 'sp', split_axis=0, concat_axis=0, tiled=True)]
    pallas_call x0 -> x3, Pallas kernels: none -> 33.8 us  [attention(): pl.pallas_call(functools.partial(kernel, rows, cols), grid=(pairs,), out_...]
    convert_element_type x9 -> x3, other arithmetic: 25.6 us -> 5.11 us  [body(): (current.astype(jnp.float32) + update.astype(jnp.float32)).astype(jnp.bfl...]
    ppermute x21 -> x6, starting transfers between devices: 29.2 us -> 12.9 us  [the longest x3 12.9 us: body(): right = lax.ppermute(keyval[:, :half_c], 'sp', to_left)]
    dot_general x9 -> x12, matrix products: 38.5 us -> 38.2 us  [the longest x9 25.6 us: project(): product = jnp.dot(scaled, weight[layer], preferred_element_type=jnp.float32)]
  transfers between devices with their start and end apart: 27 -> 12, of which waited for: 15 -> 12; matrix products, arithmetic and copies ran while one was open for 3% -> 3% of each run, Pallas kernels for 0% -> 0%
where the time goes in v1:
time: 321 us
  waiting for transfers between devices  165 us (51%)
  blocking collectives  41.4 us (13%)
  matrix products  38.2 us (12%)
  Pallas kernels  33.8 us (11%)
  between operations  13.7 us (4%)
  starting transfers between devices  13.1 us (4%)
  other arithmetic  12.4 us (4%)
    reduce_scatter x3, waiting for transfers between devices, body(): update = lax.psum_scatter(partial, 'tp', scatter_dimension=1, tiled=True)  83.2 us
    all_gather x3, waiting for transfers between devices, body(): raw = lax.all_gather(current, 'tp', axis=1, tiled=True).astype(jnp.float32)  66.6 us
    pallas_call x3, Pallas kernels, attention(): pl.pallas_call(functools.partial(kernel, rows, cols), grid=(pairs,), out_...  33.8 us
    dot_general x9, matrix products, project(): product = jnp.dot(scaled, weight[layer], preferred_element_type=jnp.float32)  25.6 us
    all_to_all x1, blocking collectives, body(): lax.all_to_all(turned, 'sp', split_axis=0, concat_axis=0, tiled=True)  21.7 us
    all_to_all x1, blocking collectives, body(): lax.all_to_all(current, 'sp', split_axis=0, concat_axis=0, tiled=True)  19.7 us
    ppermute x3, waiting for transfers between devices, body(): left = lax.ppermute(keyval[:, cols - half_c:], 'sp', to_right)  14.7 us
    ppermute x3, starting transfers between devices, body(): right = lax.ppermute(keyval[:, :half_c], 'sp', to_left)  12.9 us
  transfers between devices with their start and end apart: 12, of which 12 were waited for; matrix products, arithmetic and copies ran while one was open for 3% of the time, Pallas kernels for 0%

profile of v1, /device:TPU:0, one launch (start us, length us, event | category | flops | bytes accessed | tf_op | source)
XLA Modules:
  0.0 320.6 jit_solution(14276262111966332749)
XLA Ops:
  6.5 0.0 all-gather.4.cloned.1.call-start
  6.5 1.3 copy.16
  7.8 21.7 %all_to_all.21 = bf16[8,64,512]{2,1,0:T(8,128)(2,1)} all-to-all(bf16[8,64,512]{2,1,0:T(8,128)(2,1)S(1)} %bitcast.115), channel_id=1, replica_groups=mesh['sp'=8,'tp'=4] {'sp'}, dimensions={0} | all-to-all | bytes 1048576 | tf_op jit(solution)/shard_map/all_to_all | solution.py:144
  29.5 0.0 all-gather.4.cloned.1.call-update
  29.6 0.0 reduce-scatter.4.cloned.1.call-start
  29.6 0.0 copy-done.6
  29.6 0.1 slice.85
  29.7 0.1 rev.4
  29.8 0.1 pad.9.clone
  29.9 0.1 pad_maximum_fusion.6
  30.0 0.0 copy-done.7
  30.1 21.3 %all-gather.4.cloned.1.call-done = bf16[512,2048]{1,0:T(8,128)(2,1)} async-done(((bf16[512,512]{1,0:T(8,128)(2,1)}), bf16[512,2048]{1,0:T(8,128)(2,1)}) %all-gather.4.cloned.1.call-update) | async-done | bytes 2097168 | tf_op jit(solution)/shard_map/all_gather | solution.py:149
  51.3 2.2 fusion.1
  53.6 2.8 fusion.128.k_ref
  56.4 2.8 fusion.123.v_ref
  59.3 0.1 pad_maximum_fusion
  59.4 4.3 %collective-permute-start.1 = (bf16[8,8,1024]{2,1,0:T(8,128)(2,1)S(1)}, bf16[8,8,1024]{2,1,0:T(8,128)(2,1)S(1)}, u32[]{:S(2)}, u32[]{:S(2)}) collective-permute-start(bf16[8,8,1024]{2,1,0:T(8,128)(2,1)S(1)} %get-tuple-element.10), channel_id=1, source_target_pairs={{0,28},{4,0},{8,4},{12,8},{16,12},{20,16},{24,20},{28,24},{1,29},{... | collective-permute-start | bytes 393224 | tf_op jit(solution)/shard_map/ppermute | solution.py:161
  63.7 0.0 collective-permute-start
  63.7 2.8 fusion.138.q_ref
  66.6 0.3 collective-permute-done.1
  66.9 4.9 %collective-permute-done = bf16[8,8,1024]{2,1,0:T(8,128)(2,1)S(1)} collective-permute-done((bf16[8,8,1024]{2,1,0:T(8,128)(2,1)S(1)}, bf16[8,8,1024]{2,1,0:T(8,128)(2,1)S(1)}, u32[]{:S(2)}, u32[]{:S(2)}) %collective-permute-start) | collective-permute-done | bytes 131104 | tf_op jit(solution)/shard_map/ppermute | solution.py:160
  71.8 11.3 %window_attention.3 = bf16[512,512]{1,0:T(8,128)(2,1)S(1)} custom-call(bf16[512,512]{1,0:T(8,128)(2,1)S(1)} %fusion.138.q_ref, bf16[512,512]{1,0:T(8,128)(2,1)S(1)} %fusion.128.k_ref, bf16[512,512]{1,0:T(8,128)(2,1)S(1)} %fusion.123.v_ref, bf16[128,1024]{1,0:T(8,128)(2,1)S(1)} %bitcast.108, bf16[128,1024]{1,0:T(8,128)(2,1)S(1)} %bitcast.109, ...), custom_call_target="tpu_custom_call" | custom-call | tf_op jit(solution)/shard_map/window_attention/pallas_call | solution.py:107
  83.1 4.2 %convolution_convert_fusion.2 = bf16[512,2048]{1,0:T(8,128)(2,1)} fusion(bf16[512,512]{1,0:T(8,128)(2,1)S(1)} %window_attention.3, bf16[3,512,2048]{2,1,0:T(8,128)(2,1)} %param.12), kind=kOutput, calls=%fused_computation.14 | convolution fusion | flops 1074790400 | bytes 4718592 | tf_op jit(solution)/shard_map/dot_general | solution.py:165
  87.3 0.0 reduce-scatter.4.cloned.1.call-update
  87.3 0.0 all-gather.6.cloned.1.call-start
  87.3 27.7 %reduce-scatter.4.cloned.1.call-done = bf16[512,512]{1,0:T(8,128)(2,1)} async-done(((bf16[512,2048]{1,0:T(8,128)(2,1)}), bf16[512,512]{1,0:T(8,128)(2,1)}) %reduce-scatter.4.cloned.1.call-update) | async-done | bytes 524304 | tf_op jit(solution)/shard_map/reduce_scatter | solution.py:166
  115.1 2.0 add_convert_fusion.2
  117.0 0.0 all-gather.6.cloned.1.call-update
  117.1 0.0 reduce-scatter.6.cloned.1.call-start
  117.1 22.6 %all-gather.6.cloned.1.call-done = bf16[512,2048]{1,0:T(8,128)(2,1)} async-done(((bf16[512,512]{1,0:T(8,128)(2,1)}), bf16[512,2048]{1,0:T(8,128)(2,1)}) %all-gather.6.cloned.1.call-update) | async-done | bytes 2097168 | tf_op jit(solution)/shard_map/all_gather | solution.py:149
  139.8 2.2 fusion.3
  142.0 2.8 fusion.113.k_ref
  144.9 2.9 fusion.108.v_ref
  147.7 0.1 pad_maximum_fusion.1
  147.9 4.3 %collective-permute-start.3 = (bf16[8,8,1024]{2,1,0:T(8,128)(2,1)S(1)}, bf16[8,8,1024]{2,1,0:T(8,128)(2,1)S(1)}, u32[]{:S(2)}, u32[]{:S(2)}) collective-permute-start(bf16[8,8,1024]{2,1,0:T(8,128)(2,1)S(1)} %get-tuple-element.8), channel_id=1, source_target_pairs={{0,28},{4,0},{8,4},{12,8},{16,12},{20,16},{24,20},{28,24},{1,29},{... | collective-permute-start | bytes 393224 | tf_op jit(solution)/shard_map/ppermute | solution.py:161
  152.2 0.0 collective-permute-start.2
  152.2 2.8 fusion.143.q_ref
  155.0 0.3 collective-permute-done.3
  155.3 4.9 %collective-permute-done.2 = bf16[8,8,1024]{2,1,0:T(8,128)(2,1)S(1)} collective-permute-done((bf16[8,8,1024]{2,1,0:T(8,128)(2,1)S(1)}, bf16[8,8,1024]{2,1,0:T(8,128)(2,1)S(1)}, u32[]{:S(2)}, u32[]{:S(2)}) %collective-permute-start.2) | collective-permute-done | bytes 131104 | tf_op jit(solution)/shard_map/ppermute | solution.py:160
  160.2 11.3 %window_attention.4 = bf16[512,512]{1,0:T(8,128)(2,1)S(1)} custom-call(bf16[512,512]{1,0:T(8,128)(2,1)S(1)} %fusion.143.q_ref, bf16[512,512]{1,0:T(8,128)(2,1)S(1)} %fusion.113.k_ref, bf16[512,512]{1,0:T(8,128)(2,1)S(1)} %fusion.108.v_ref, bf16[128,1024]{1,0:T(8,128)(2,1)S(1)} %bitcast.110, bf16[128,1024]{1,0:T(8,128)(2,1)S(1)} %bitcast.111, ...), custom_call_target="tpu_custom_call" | custom-call | tf_op jit(solution)/shard_map/window_attention/pallas_call | solution.py:107
  171.5 4.2 %convolution_convert_fusion.1 = bf16[512,2048]{1,0:T(8,128)(2,1)} fusion(bf16[512,512]{1,0:T(8,128)(2,1)S(1)} %window_attention.4, bf16[3,512,2048]{2,1,0:T(8,128)(2,1)} %param.12), kind=kOutput, calls=%fused_computation.13 | convolution fusion | flops 1074790400 | bytes 4718592 | tf_op jit(solution)/shard_map/dot_general | solution.py:165
  175.7 0.0 reduce-scatter.6.cloned.1.call-update
  175.7 0.0 all-gather.8.cloned.1.call-start
  175.8 27.7 %reduce-scatter.6.cloned.1.call-done = bf16[512,512]{1,0:T(8,128)(2,1)} async-done(((bf16[512,2048]{1,0:T(8,128)(2,1)}), bf16[512,512]{1,0:T(8,128)(2,1)}) %reduce-scatter.6.cloned.1.call-update) | async-done | bytes 524304 | tf_op jit(solution)/shard_map/reduce_scatter | solution.py:166
  203.5 2.0 add_convert_fusion.1
  205.5 0.0 all-gather.8.cloned.1.call-update
  205.5 0.0 reduce-scatter.8.cloned.1.call-start
  205.5 22.7 %all-gather.8.cloned.1.call-done = bf16[512,2048]{1,0:T(8,128)(2,1)} async-done(((bf16[512,512]{1,0:T(8,128)(2,1)}), bf16[512,2048]{1,0:T(8,128)(2,1)}) %all-gather.8.cloned.1.call-update) | async-done | bytes 2097168 | tf_op jit(solution)/shard_map/all_gather | solution.py:149
  228.2 2.2 fusion.5
  230.4 2.8 fusion.98.k_ref
  233.3 2.8 fusion.93.v_ref
  236.1 0.1 pad_maximum_fusion.2
  236.3 4.3 %collective-permute-start.5 = (bf16[8,8,1024]{2,1,0:T(8,128)(2,1)S(1)}, bf16[8,8,1024]{2,1,0:T(8,128)(2,1)S(1)}, u32[]{:S(2)}, u32[]{:S(2)}) collective-permute-start(bf16[8,8,1024]{2,1,0:T(8,128)(2,1)S(1)} %get-tuple-element.6), channel_id=1, source_target_pairs={{0,28},{4,0},{8,4},{12,8},{16,12},{20,16},{24,20},{28,24},{1,29},{... | collective-permute-start | bytes 393224 | tf_op jit(solution)/shard_map/ppermute | solution.py:161
  240.6 0.0 collective-permute-start.4
  240.6 2.8 fusion.148.q_ref
  243.4 0.3 collective-permute-done.5
  243.7 4.9 %collective-permute-done.4 = bf16[8,8,1024]{2,1,0:T(8,128)(2,1)S(1)} collective-permute-done((bf16[8,8,1024]{2,1,0:T(8,128)(2,1)S(1)}, bf16[8,8,1024]{2,1,0:T(8,128)(2,1)S(1)}, u32[]{:S(2)}, u32[]{:S(2)}) %collective-permute-start.4) | collective-permute-done | bytes 131104 | tf_op jit(solution)/shard_map/ppermute | solution.py:160
  248.6 11.3 %window_attention.5 = bf16[512,512]{1,0:T(8,128)(2,1)S(1)} custom-call(bf16[512,512]{1,0:T(8,128)(2,1)S(1)} %fusion.148.q_ref, bf16[512,512]{1,0:T(8,128)(2,1)S(1)} %fusion.98.k_ref, bf16[512,512]{1,0:T(8,128)(2,1)S(1)} %fusion.93.v_ref, bf16[128,1024]{1,0:T(8,128)(2,1)S(1)} %bitcast.106, bf16[128,1024]{1,0:T(8,128)(2,1)S(1)} %bitcast.107, ...), custom_call_target="tpu_custom_call" | custom-call | tf_op jit(solution)/shard_map/window_attention/pallas_call | solution.py:107
  259.9 4.2 %convolution_convert_fusion = bf16[512,2048]{1,0:T(8,128)(2,1)} fusion(bf16[512,512]{1,0:T(8,128)(2,1)S(1)} %window_attention.5, bf16[3,512,2048]{2,1,0:T(8,128)(2,1)} %param.12), kind=kOutput, calls=%fused_computation.12 | convolution fusion | flops 1074790400 | bytes 4718592 | tf_op jit(solution)/shard_map/dot_general | solution.py:165
  264.1 0.0 reduce-scatter.8.cloned.1.call-update
  264.1 27.8 %reduce-scatter.8.cloned.1.call-done = bf16[512,512]{1,0:T(8,128)(2,1)} async-done(((bf16[512,2048]{1,0:T(8,128)(2,1)}), bf16[512,512]{1,0:T(8,128)(2,1)}) %reduce-scatter.8.cloned.1.call-update) | async-done | bytes 524304 | tf_op jit(solution)/shard_map/reduce_scatter | solution.py:166
  291.9 1.2 add_convert_fusion
  293.1 19.7 %all_to_all.22 = bf16[8,64,512]{2,1,0:T(8,128)(2,1)S(1)} all-to-all(bf16[8,64,512]{2,1,0:T(8,128)(2,1)S(1)} %bitcast.113), channel_id=1, replica_groups=mesh['sp'=8,'tp'=4] {'sp'}, dimensions={0} | all-to-all | bytes 1048576 | tf_op jit(solution)/shard_map/all_to_all | solution.py:168
  312.8 1.0 copy.23
  (26 shorter events, 0.2 us)
Async XLA Ops:
  6.5 23.1 %copy-start.6 = (f32[3,8,8,16]{3,2,1,0:T(8,128)S(1)}, f32[3,8,8,16]{3,2,1,0:T(8,128)}, u32[]{:S(2)}) copy-start(f32[3,8,8,16]{3,2,1,0:T(8,128)} %param.13) | copy-start | bytes 36868
  6.5 23.5 %copy-start.7 = (bf16[3,2048]{1,0:T(4,128)(2,1)S(1)}, bf16[3,2048]{1,0:T(4,128)(2,1)}, u32[]{:S(2)}) copy-start(bf16[3,2048]{1,0:T(4,128)(2,1)} %param.8) | copy-start | bytes 36868
  6.5 44.8 %all-gather.4.cloned.1.call-start = ((), (), s32[]{:S(2)}) async-start(), calls=%async_computation.5 | async-start | bytes 2621440 | tf_op jit(solution)/shard_map/all_gather | solution.py:149
  29.6 85.5 %reduce-scatter.4.cloned.1.call-start = ((), (), s32[]{:S(2)}) async-start(), calls=%async_computation.6 | async-start | bytes 2621440 | tf_op jit(solution)/shard_map/reduce_scatter | solution.py:166
  51.3 2.2 copy-start.3
  59.4 7.4 %collective-permute-start.1 = (bf16[8,8,1024]{2,1,0:T(8,128)(2,1)S(1)}, bf16[8,8,1024]{2,1,0:T(8,128)(2,1)S(1)}, u32[]{:S(2)}, u32[]{:S(2)}) collective-permute-start(bf16[8,8,1024]{2,1,0:T(8,128)(2,1)S(1)} %get-tuple-element.10), channel_id=1, source_target_pairs={{0,28},{4,0},{8,4},{12,8},{16,12},{20,16},{24,20},{28,24},{1,29},{... | collective-permute-start | bytes 393224 | tf_op jit(solution)/shard_map/ppermute | solution.py:161
  63.7 8.0 %collective-permute-start = (bf16[8,8,1024]{2,1,0:T(8,128)(2,1)S(1)}, bf16[8,8,1024]{2,1,0:T(8,128)(2,1)S(1)}, u32[]{:S(2)}, u32[]{:S(2)}) collective-permute-start(bf16[8,8,1024]{2,1,0:T(8,128)(2,1)S(1)} %get-tuple-element.9), channel_id=1, source_target_pairs={{0,4},{4,8},{8,12},{12,16},{16,20},{20,24},{24,28},{28,0},{1,5},{5... | collective-permute-start | bytes 393224 | tf_op jit(solution)/shard_map/ppermute | solution.py:160
  87.3 27.8 %copy-start.2 = (bf16[8,64,512]{2,1,0:T(8,128)(2,1)S(1)}, bf16[8,64,512]{2,1,0:T(8,128)(2,1)}, u32[]{:S(2)}) copy-start(bf16[8,64,512]{2,1,0:T(8,128)(2,1)} %all_to_all.21) | copy-start | bytes 1572868
  87.3 52.5 %all-gather.6.cloned.1.call-start = ((), (), s32[]{:S(2)}) async-start(), calls=%async_computation.7 | async-start | bytes 2621440 | tf_op jit(solution)/shard_map/all_gather | solution.py:149
  117.1 86.4 %reduce-scatter.6.cloned.1.call-start = ((), (), s32[]{:S(2)}) async-start(), calls=%async_computation.8 | async-start | bytes 2621440 | tf_op jit(solution)/shard_map/reduce_scatter | solution.py:166
  139.8 2.2 copy-start.5
  147.9 7.4 %collective-permute-start.3 = (bf16[8,8,1024]{2,1,0:T(8,128)(2,1)S(1)}, bf16[8,8,1024]{2,1,0:T(8,128)(2,1)S(1)}, u32[]{:S(2)}, u32[]{:S(2)}) collective-permute-start(bf16[8,8,1024]{2,1,0:T(8,128)(2,1)S(1)} %get-tuple-element.8), channel_id=1, source_target_pairs={{0,28},{4,0},{8,4},{12,8},{16,12},{20,16},{24,20},{28,24},{1,29},{... | collective-permute-start | bytes 393224 | tf_op jit(solution)/shard_map/ppermute | solution.py:161
  152.2 8.0 %collective-permute-start.2 = (bf16[8,8,1024]{2,1,0:T(8,128)(2,1)S(1)}, bf16[8,8,1024]{2,1,0:T(8,128)(2,1)S(1)}, u32[]{:S(2)}, u32[]{:S(2)}) collective-permute-start(bf16[8,8,1024]{2,1,0:T(8,128)(2,1)S(1)} %get-tuple-element.7), channel_id=1, source_target_pairs={{0,4},{4,8},{8,12},{12,16},{16,20},{20,24},{24,28},{28,0},{1,5},{5... | collective-permute-start | bytes 393224 | tf_op jit(solution)/shard_map/ppermute | solution.py:160
  175.7 27.8 %copy-start = (bf16[512,512]{1,0:T(8,128)(2,1)S(1)}, bf16[512,512]{1,0:T(8,128)(2,1)}, u32[]{:S(2)}) copy-start(bf16[512,512]{1,0:T(8,128)(2,1)} %add_convert_fusion.2) | copy-start | bytes 1572868
  175.7 52.5 %all-gather.8.cloned.1.call-start = ((), (), s32[]{:S(2)}) async-start(), calls=%async_computation.9 | async-start | bytes 2621440 | tf_op jit(solution)/shard_map/all_gather | solution.py:149
  205.5 86.4 %reduce-scatter.8.cloned.1.call-start = ((), (), s32[]{:S(2)}) async-start(), calls=%async_computation.10 | async-start | bytes 2621440 | tf_op jit(solution)/shard_map/reduce_scatter | solution.py:166
  228.2 2.2 copy-start.4
  236.3 7.4 %collective-permute-start.5 = (bf16[8,8,1024]{2,1,0:T(8,128)(2,1)S(1)}, bf16[8,8,1024]{2,1,0:T(8,128)(2,1)S(1)}, u32[]{:S(2)}, u32[]{:S(2)}) collective-permute-start(bf16[8,8,1024]{2,1,0:T(8,128)(2,1)S(1)} %get-tuple-element.6), channel_id=1, source_target_pairs={{0,28},{4,0},{8,4},{12,8},{16,12},{20,16},{24,20},{28,24},{1,29},{... | collective-permute-start | bytes 393224 | tf_op jit(solution)/shard_map/ppermute | solution.py:161
  240.6 8.0 %collective-permute-start.4 = (bf16[8,8,1024]{2,1,0:T(8,128)(2,1)S(1)}, bf16[8,8,1024]{2,1,0:T(8,128)(2,1)S(1)}, u32[]{:S(2)}, u32[]{:S(2)}) collective-permute-start(bf16[8,8,1024]{2,1,0:T(8,128)(2,1)S(1)} %get-tuple-element.5), channel_id=1, source_target_pairs={{0,4},{4,8},{8,12},{12,16},{16,20},{20,24},{24,28},{28,0},{1,5},{5... | collective-permute-start | bytes 393224 | tf_op jit(solution)/shard_map/ppermute | solution.py:160
  264.1 27.8 %copy-start.1 = (bf16[512,512]{1,0:T(8,128)(2,1)S(1)}, bf16[512,512]{1,0:T(8,128)(2,1)}, u32[]{:S(2)}) copy-start(bf16[512,512]{1,0:T(8,128)(2,1)} %add_convert_fusion.1) | copy-start | bytes 1572868
Sparse Core Ops, SparseCore 0:
  29.7 21.5 all-gather.3
  87.4 27.6 reduce-scatter.3
  117.2 22.5 all-gather.5
  175.9 27.5 reduce-scatter.5
  205.6 22.5 all-gather.7
  264.3 27.6 reduce-scatter.7
